TPU v7x, 32 devices: a whole 2x2x4 slice. The times are simulated.
32 devices in a mesh: ep: 8 (over z, x), tp: 4 (over y, core).
Axes of the slice: x: 2, y: 2, z: 4, core: 2. Of those that a mesh axis runs over, the one named last changes fastest.
Arguments:
- mix_input: bfloat16 [3072, 2048], P('ep', 'tp'), may hold values from -6 to 6
- mix_gain: float32 [2048], replicated, may hold values from 0.1 to 1.9
- gate_b_weight: bfloat16 [2048, 2048], P(None, 'tp'), may hold values from -0.125 to 0.125
- gate_c_weight: bfloat16 [2048, 2048], P(None, 'tp'), may hold values from -0.125 to 0.125
- value_weight: bfloat16 [2048, 2048], P(None, 'tp'), may hold values from -0.125 to 0.125
- conv_weight: float32 [3, 2048], P(None, 'tp'), may hold values from -3 to 3
- out_weight: bfloat16 [2048, 2048], P('tp'), may hold values from -0.125 to 0.125
- expert_input: bfloat16 [1280, 2048], P('ep', 'tp'), may hold values from -6 to 6
- expert_gain: float32 [2048], replicated, may hold values from 0.1 to 1.9
- routes: int32 [1280, 2], P('ep'), may hold values from 0 to 7, all different within a row; in each aligned block of 160 rows (0 to 159, 160 to 319, ...) at most 80 rows name the same one
- route_weight: float32 [1280, 2], P('ep'), may hold values from 0.2 to 1
- expert_gate: bfloat16 [8, 2048, 3072], P('ep', None, 'tp'), may hold values from -0.125 to 0.125
- expert_up: bfloat16 [8, 2048, 3072], P('ep', None, 'tp'), may hold values from -0.125 to 0.125
- expert_down: bfloat16 [8, 3072, 2048], P('ep', 'tp'), may hold values from -0.109375 to 0.109375
Outputs:
- mix_output: bfloat16 [3072, 2048], P('ep', 'tp')
- expert_output: bfloat16 [1280, 2048], P('ep', 'tp')
Inputs may be any that keep to these rules, and one draw needn't show every extreme that they name: `routes`: the 2 experts of a row differ. Among the rows of one device no expert is named more than 80 times, a bound that some block reaches.
All inputs are finite; a program needn't handle non-finite values.
Results may differ from a plain program's by a relative error of at most 0.019.
Values may be sent and summed in bfloat16 or wider, within the bound.
A program may use at most 64 MiB of HBM per device.

v0:
```python
import functools

import jax
import jax.numpy as jnp
from jax import lax
from jax.experimental import pallas as pl
from jax.experimental.pallas import tpu as pltpu
from jax.sharding import PartitionSpec as P

MESH = pl.DeviceIdType.MESH
epsilon = 1e-06
routed_scale = 2.5
f32 = jnp.float32
bf16 = jnp.bfloat16


def kernel(
    dims,
    mix_ref, mgain_ref, wb_hbm, wc_hbm, wv_hbm, conv_ref, wo_hbm,
    exp_ref, egain_ref, routes_ref, rw_ref, wg_hbm, wu_hbm, wd_hbm,
    mo_ref, eo_ref,
    wb, wc, wv, wo, wg, wu, wd, w_sem,
    tables, outg, xg, xs, fac, outer, prod, edge, gated, pm, rm, sm, ym,
    xe, xes, efac, act, pe, re, se, yr, fin, ret,
    mys, myr, mps, mpr, eps, epr, eys, eyr, pps, ppr, edges,
    rms, rmr, yms, ymr, res, rer, ses, ser, rts, rtr,
):
    n_ep, n_tp, cap, group = dims
    chips = n_tp // 2
    n_group = n_ep // group
    rows, feat = mix_ref.shape
    width = feat * n_tp
    tok = exp_ref.shape[0]
    slots = n_ep * cap
    half = n_ep // 2
    e = lax.axis_index("ep")
    t = lax.axis_index("tp")
    y, c = lax.div(t, 2), lax.rem(t, 2)
    partner = y * 2 + 1 - c
    home = lax.div(e, group)

    def cols(b):
        return pl.ds(pl.multiple_of(b * feat, feat), feat)

    def remote(src, dst, send_sem, recv_sem, ep, tp):
        return pltpu.make_async_remote_copy(
            src_ref=src, dst_ref=dst, send_sem=send_sem, recv_sem=recv_sem,
            device_id=(ep, tp), device_id_type=MESH,
        )

    def ahead(dy):
        return lax.rem(y + dy, chips) * 2 + c

    def behind(dy):
        return lax.rem(y - dy + chips, chips) * 2 + c

    def loop(count, body, start=0):
        lax.fori_loop(start, count, lambda i, carry: (body(i), carry)[1], 0)

    def mix_y(dy):
        return remote(mix_ref, xg.at[:, cols(t)], mys.at[dy], myr.at[dy], e, ahead(dy))

    def mix_p():
        return remote(mix_ref, xg.at[:, cols(t)], mps.at[0], mpr.at[0], e, partner)

    def mix_f(dy):
        part = xg.at[:, cols(behind(dy))]
        return remote(part, part, mps.at[dy], mpr.at[dy], e, partner)

    def dispatch(d):
        s = lax.rem(e + d, n_ep)
        return remote(outg.at[s], xe.at[e, :, cols(t)], eps.at[d], epr.at[d], s, t)

    def span_in(i):
        return pl.ds(lax.rem(home - i + n_group, n_group) * group, group)

    def exp_y(i, dy):
        part = xe.at[span_in(i), :, cols(t)]
        return remote(part, part, eys.at[dy, i], eyr.at[dy, i], e, ahead(dy))

    def exp_p(i):
        part = xe.at[span_in(i), :, cols(t)]
        return remote(part, part, pps.at[0, i], ppr.at[0, i], e, partner)

    def exp_f(i, dy):
        part = xe.at[span_in(i), :, cols(behind(dy))]
        return remote(part, part, pps.at[dy, i], ppr.at[dy, i], e, partner)

    def edge_copy():
        return remote(
            prod.at[pl.ds(rows, 8)], edge, edges.at[0], edges.at[1], lax.rem(e + 1, n_ep), t
        )

    def mix_half(q):
        return remote(pm.at[q * 2 + 1 - c], rm.at[q], rms.at[q], rmr.at[q], e, partner)

    def mix_sum(dy):
        return remote(sm.at[dy], ym.at[dy], yms.at[dy], ymr.at[dy], e, ahead(dy))

    def exp_half(q, h):
        at = pl.ds(h * half, half)
        return remote(
            pe.at[q * 2 + 1 - c, at], re.at[q, at], res.at[h, q], rer.at[h, q], e, partner
        )

    def span_out(i):
        return pl.ds(i * group, group)

    def source(p):
        return lax.rem(home - lax.div(p, group) + n_group, n_group) * group + lax.rem(p, group)

    def place(s):
        turn = lax.rem(home - lax.div(s, group) + n_group, n_group)
        return turn * group + lax.rem(s, group)

    def exp_sum(i, dy):
        return remote(
            se.at[dy, span_out(i)], yr.at[dy, span_out(i)],
            ses.at[dy, i], ser.at[dy, i], e, ahead(dy),
        )

    def back(d):
        s = lax.rem(e + d, n_ep)
        return remote(fin.at[place(s)], ret.at[e], rts.at[d], rtr.at[d], s, t)

    loads = [
        pltpu.make_async_copy(src, dst, w_sem.at[i])
        for i, (src, dst) in enumerate(
            ((wb_hbm, wb), (wc_hbm, wc), (wv_hbm, wv), (wo_hbm, wo),
             (wg_hbm, wg), (wu_hbm, wu), (wd_hbm, wd))
        )
    ]
    for load in loads:
        load.start()

    barrier = pltpu.get_barrier_semaphore()
    for dy in range(1, chips):
        pl.semaphore_signal(barrier, inc=1, device_id=(e, ahead(dy)), device_id_type=MESH)
    pl.semaphore_signal(barrier, inc=1, device_id=(e, partner), device_id_type=MESH)

    def greet(d):
        pl.semaphore_signal(
            barrier, inc=1, device_id=(lax.rem(e + d + 1, n_ep), t), device_id_type=MESH
        )

    loop(n_ep - 1, greet)

    row = lax.broadcasted_iota(jnp.int32, (tok, tok), 0)
    column = lax.broadcasted_iota(jnp.int32, (tok, tok), 1)

    def upright(line):
        return jnp.sum(jnp.where(row == column, line, 0.0), axis=1, keepdims=True)

    lane = lax.broadcasted_iota(jnp.int32, (tok, 128), 1).astype(f32)
    chosen = [upright(routes_ref[k : k + 1, :].astype(f32)) for k in range(2)]
    named = [chosen[k] == lane for k in range(2)]
    either = jnp.where(named[0] | named[1], 1.0, 0.0).astype(bf16)
    before = row > column
    counts = jnp.dot(
        jnp.where(before, 1.0, 0.0).astype(bf16), either, preferred_element_type=f32
    )
    slot_iota = lax.broadcasted_iota(jnp.int32, (tok, slots), 1).astype(f32)
    both = []
    for k in range(2):
        rank = jnp.sum(jnp.where(named[k], counts, 0.0), axis=1, keepdims=True)
        slot = chosen[k] * float(cap) + rank
        one = jnp.where(slot_iota == slot, 1.0, 0.0)
        tables[k] = one.astype(bf16)
        both.append(one)
    send = (both[0] + both[1]).astype(bf16)
    outg[...] = (
        lax.dot_general(
            send, exp_ref[...], (((0,), (0,)), ((), ())), preferred_element_type=f32
        )
        .astype(bf16)
        .reshape(n_ep, cap, feat)
    )

    pl.semaphore_wait(barrier, n_ep - 1 + chips)

    loop(n_ep - 1, lambda d: dispatch(d + 1).start())
    for dy in range(1, chips):
        mix_y(dy).start()
    mix_p().start()
    xe[e, :, cols(t)] = outg[e]
    xg[:, cols(t)] = mix_ref[...]

    def pass_on(i):
        first = lax.rem(home - i + n_group, n_group) * group
        for j in range(group):
            d = lax.rem(e - first - j + n_ep, n_ep)

            @pl.when(d != 0)
            def _():
                dispatch(d).wait_recv()

        for dy in range(1, chips):
            exp_y(i, dy).start()
        exp_p(i).start()

    early = n_group * 5 // 8
    loop(early, pass_on)

    for dy in range(1, chips):
        mix_y(dy).wait_recv()
        mix_f(dy).start()
    mix_p().wait_recv()
    for dy in range(1, chips):
        mix_f(dy).wait_recv()

    tile = 32

    def scale_mix(i):
        at = pl.ds(pl.multiple_of(i * tile, tile), tile)
        x = xg[at].astype(f32)
        fac[at] = lax.rsqrt(jnp.sum(x * x, axis=1, keepdims=True) / width + epsilon)
        xs[at] = (x * mgain_ref[...]).astype(bf16)

    loop(rows // tile, scale_mix)
    for load in loads[:3]:
        load.wait()
    wide = 256 if feat % 256 == 0 else feat

    def project(i):
        at = pl.ds(pl.multiple_of(i * wide, wide), wide)
        x = xs[...]
        factor = fac[...]
        inner = jnp.dot(x, wc[:, at], preferred_element_type=f32) * factor
        values = jnp.dot(x, wv[:, at], preferred_element_type=f32) * factor
        prod[pl.ds(8, rows), at] = inner * values
        outer[:, at] = jnp.dot(x, wb[:, at], preferred_element_type=f32) * factor

    loop(feat // wide, project)
    edge_copy().start()
    loop(n_group, pass_on, early)

    def relay(i):
        for dy in range(1, chips):
            exp_y(i, dy).wait_recv()
            exp_f(i, dy).start()

    def arrive(i):
        exp_p(i).wait_recv()
        for dy in range(1, chips):
            exp_f(i, dy).wait_recv()

    def scale_exp(p):
        at = pl.ds(pl.multiple_of(p * cap, cap), cap)
        x = xe[source(p)].astype(f32)
        efac[at] = lax.rsqrt(jnp.sum(x * x, axis=1, keepdims=True) / width + epsilon)
        xes[at] = (x * egain_ref[...]).astype(bf16)

    hidden = wd.shape[0]
    wide_h = 256 if hidden % 256 == 0 else hidden

    def push(i):
        at = span_out(i)
        for dy in range(1, chips):
            q = lax.rem(y + dy, chips)
            se[dy, at] = (pe[ahead(dy), at].astype(f32) + re[q, at].astype(f32)).astype(bf16)
            exp_sum(i, dy).start()

    for h in range(2):
        first, last = h * n_group // 2, (h + 1) * n_group // 2
        loop(last, relay, first)
        loop(last, arrive, first)
        loop((h + 1) * half, scale_exp, h * half)
        if h == 0:
            loads[4].wait()
            loads[5].wait()
        part = pl.ds(h * half * cap, half * cap)

        def activate(at):
            x = xes[part]
            factor = efac[part]
            gate = jnp.dot(x, wg[0, :, at], preferred_element_type=f32) * factor
            up = jnp.dot(x, wu[0, :, at], preferred_element_type=f32) * factor
            act[part, at] = (gate / (1.0 + jnp.exp(-gate)) * up).astype(bf16)

        if wide_h == hidden:
            activate(slice(None))
        else:
            loop(
                hidden // wide_h,
                lambda i: activate(pl.ds(pl.multiple_of(i * wide_h, wide_h), wide_h)),
            )
        if h == 0:
            loads[6].wait()

        def exp_down(b):
            out = jnp.dot(act[part], wd[:, cols(b)], preferred_element_type=f32)
            pe[b, pl.ds(h * half, half)] = out.astype(bf16).reshape(half, cap, feat)

        def exp_given(q):
            exp_down(q * 2 + 1 - c)
            exp_half(q, h).start()

        loop(chips, exp_given)
        loop(chips, lambda q: exp_down(q * 2 + c))
        for q in range(chips):
            exp_half(q, h).wait_recv()
        loop(last, push, first)

    edge_copy().wait_recv()
    prod[0:8] = jnp.where(e == 0, 0.0, edge[...])

    def convolve(i):
        at = pl.ds(pl.multiple_of(i * 128, 128), 128)
        convolved = (
            conv_ref[0:1, at] * prod[pl.ds(6, rows), at]
            + conv_ref[1:2, at] * prod[pl.ds(7, rows), at]
            + conv_ref[2:3, at] * prod[pl.ds(8, rows), at]
        )
        gated[:, at] = (outer[:, at] * convolved).astype(bf16)

    loop(feat // 128, convolve)
    loads[3].wait()

    def mix_down(b):
        pm[b] = jnp.dot(gated[...], wo[:, cols(b)], preferred_element_type=f32).astype(bf16)

    def mix_given(q):
        mix_down(q * 2 + 1 - c)
        mix_half(q).start()

    loop(chips, mix_given)
    loop(chips, lambda q: mix_down(q * 2 + c))
    for q in range(chips):
        mix_half(q).wait_recv()
    for dy in range(1, chips):
        q = lax.rem(y + dy, chips)
        sm[dy] = (pm[ahead(dy)].astype(f32) + rm[q].astype(f32)).astype(bf16)
        mix_sum(dy).start()

    def finish(i):
        at = span_out(i)
        whole = pe[t, at].astype(f32) + re[y, at].astype(f32)
        for dy in range(1, chips):
            exp_sum(i, dy).wait_recv()
            whole = whole + yr[dy, at].astype(f32)
        fin[at] = whole.astype(bf16)
        first = lax.rem(home - i + n_group, n_group) * group
        for j in range(group):
            d = lax.rem(first + j - e + n_ep, n_ep)

            @pl.when(d != 0)
            def _():
                back(d).start()

    loop(n_group, finish)
    ret[e] = fin[place(e)]
    loop(n_ep - 1, lambda d: back(d + 1).wait_recv())

    scores = rw_ref[...]
    normalized = scores / jnp.sum(scores, axis=0, keepdims=True) * routed_scale
    share = [upright(normalized[k : k + 1, :]) for k in range(2)]
    results = ret[...].reshape(slots, feat)
    eo_ref[...] = (
        share[0] * jnp.dot(tables[0], results, preferred_element_type=f32)
        + share[1] * jnp.dot(tables[1], results, preferred_element_type=f32)
    ).astype(bf16)

    total = pm[t].astype(f32) + rm[y].astype(f32)
    for dy in range(1, chips):
        mix_sum(dy).wait_recv()
        total = total + ym[dy].astype(f32)
    mo_ref[...] = total.astype(bf16)

    def drain(d):
        dispatch(d + 1).wait_send()
        back(d + 1).wait_send()

    loop(n_ep - 1, drain)
    mix_p().wait_send()
    edge_copy().wait_send()
    for dy in range(1, chips):
        mix_y(dy).wait_send()
        mix_f(dy).wait_send()
        mix_sum(dy).wait_send()
    for q in range(chips):
        mix_half(q).wait_send()
        exp_half(q, 0).wait_send()
        exp_half(q, 1).wait_send()

    def drain_groups(i):
        exp_p(i).wait_send()
        for dy in range(1, chips):
            exp_y(i, dy).wait_send()
            exp_f(i, dy).wait_send()
            exp_sum(i, dy).wait_send()

    loop(n_group, drain_groups)


def solution(mesh):
    n_ep, n_tp = mesh.shape["ep"], mesh.shape["tp"]
    chips = n_tp // 2

    def local(
        mix_input, mix_gain, gate_b, gate_c, value_w, conv_weight, out_weight,
        expert_input, expert_gain, routes, route_weight, expert_gate, expert_up, expert_down,
    ):
        rows, feat = mix_input.shape
        width = feat * n_tp
        tok, top = routes.shape
        experts = n_ep * expert_gate.shape[0]
        assert expert_gate.shape[0] == 1 and top == 2
        cap = -(-(2 * tok * top // experts) // 16) * 16
        hidden = expert_gate.shape[2]
        group = max(1, n_ep // 8)
        n_group = n_ep // group
        slots = n_ep * cap
        vm, sem = pltpu.VMEM, pltpu.SemaphoreType.DMA
        scratch = [
            vm((width, feat), bf16), vm((width, feat), bf16), vm((width, feat), bf16),
            vm((feat, width), bf16),
            vm((1, width, hidden), bf16), vm((1, width, hidden), bf16), vm((hidden, width), bf16),
            sem((7,)),
            vm((2, tok, slots), bf16), vm((n_ep, cap, feat), bf16),
            vm((rows, width), bf16), vm((rows, width), bf16), vm((rows, 1), f32),
            vm((rows, feat), f32), vm((rows + 8, feat), f32), vm((8, feat), f32),
            vm((rows, feat), bf16),
            vm((n_tp, rows, feat), bf16), vm((chips, rows, feat), bf16),
            vm((chips, rows, feat), bf16), vm((chips, rows, feat), bf16),
            vm((n_ep, cap, width), bf16), vm((slots, width), bf16), vm((slots, 1), f32),
            vm((slots, hidden), bf16),
            vm((n_tp, n_ep, cap, feat), bf16), vm((chips, n_ep, cap, feat), bf16),
            vm((chips, n_ep, cap, feat), bf16), vm((chips, n_ep, cap, feat), bf16),
            vm((n_ep, cap, feat), bf16), vm((n_ep, cap, feat), bf16),
            sem((chips,)), sem((chips,)), sem((chips,)), sem((chips,)),
            sem((n_ep,)), sem((n_ep,)),
            sem((chips, n_group)), sem((chips, n_group)),
            sem((chips, n_group)), sem((chips, n_group)),
            sem((2,)),
            sem((chips,)), sem((chips,)), sem((chips,)), sem((chips,)),
            sem((2, chips)), sem((2, chips)),
            sem((chips, n_group)), sem((chips, n_group)),
            sem((n_ep,)), sem((n_ep,)),
        ]
        v = pl.BlockSpec(memory_space=pltpu.VMEM)
        a = pl.BlockSpec(memory_space=pl.ANY)
        return pl.pallas_call(
            functools.partial(kernel, (n_ep, n_tp, cap, group)),
            out_shape=(
                jax.ShapeDtypeStruct((rows, feat), bf16),
                jax.ShapeDtypeStruct((tok, feat), bf16),
            ),
            in_specs=[v, v, a, a, a, v, a, v, v, v, v, a, a, a],
            out_specs=(v, v),
            scratch_shapes=scratch,
            compiler_params=pltpu.CompilerParams(
                collective_id=0, has_side_effects=True, vmem_limit_bytes=62 << 20
            ),
        )(
            mix_input, mix_gain.reshape(1, -1), gate_b, gate_c, value_w, conv_weight, out_weight,
            expert_input, expert_gain.reshape(1, -1), routes.T, route_weight.T,
            expert_gate, expert_up, expert_down.reshape(hidden, width),
        )

    in_specs = (
        P("ep", "tp"), P(), P(None, "tp"), P(None, "tp"), P(None, "tp"), P(None, "tp"),
        P("tp", None), P("ep", "tp"), P(), P("ep", None), P("ep", None),
        P("ep", None, "tp"), P("ep", None, "tp"), P("ep", "tp", None),
    )
    out_specs = (P("ep", "tp"), P("ep", "tp"))
    return jax.shard_map(local, mesh=mesh, in_specs=in_specs, out_specs=out_specs, check_vma=False)
```

profile of v0, /device:TPU:0, one launch (start us, length us, event | category | flops | bytes accessed | tf_op | source)
XLA Modules:
  0.0 67.5 jit_solution(9519356107450748406)
XLA Ops:
  0.6 63.5 %shard_map.149 = (bf16[384,512]{1,0:T(8,128)(2,1)}, bf16[160,512]{1,0:T(8,128)(2,1)}) custom-call(bf16[384,512]{1,0:T(8,128)(2,1)} %mix_ref.1, f32[1,2048]{1,0:T(1,128)} %bitcast.6, bf16[2048,512]{1,0:T(8,128)(2,1)} %wb_hbm.1, bf16[2048,512]{1,0:T(8,128)(2,1)} %wc_hbm.1, bf16[2048,512]{1,0:T(8,128)(2,1)} %wv_hbm.1, f32[3,512]{1,0:T(4,128)} %conv_ref.1, ...), custom_call_target="tpu_custom_call" | custom-call | tf_op jit(solution)/shard_map/pallas_call | solution.py:442
  64.2 1.8 %copy.18 = bf16[384,512]{1,0:T(8,128)(2,1)} copy(bf16[384,512]{1,0:T(8,128)(2,1)} %get-tuple-element.4) | data formatting | bytes 786432
  65.9 1.6 %copy.19 = bf16[160,512]{1,0:T(8,128)(2,1)} copy(bf16[160,512]{1,0:T(8,128)(2,1)} %get-tuple-element.5) | data formatting | bytes 327680
where the time goes:
time: 67.7 us; the launch traced here: 67.5 us
  Pallas kernels  63.5 us (94%)
  local copies, waits for them, and re-layouts  3.36 us (5%)
    pallas_call x1, Pallas kernels, local(): pl.pallas_call(functools.partial(kernel, (n_ep, n_tp, cap, group)), out_s...  63.5 us
    unnamed x2, local copies, waits for them, and re-layouts  3.36 us

commit v1 on v0

v1 whole, which is shorter than its diff:
```python
import functools

import jax
import jax.numpy as jnp
from jax import lax
from jax.experimental import pallas as pl
from jax.experimental.pallas import tpu as pltpu
from jax.sharding import PartitionSpec as P

MESH = pl.DeviceIdType.MESH
epsilon = 1e-06
routed_scale = 2.5
near = 4
f32 = jnp.float32
bf16 = jnp.bfloat16


def kernel(
    dims,
    mix_ref, mgain_ref, wb_hbm, wc_hbm, wv_hbm, conv_ref, wo_hbm,
    exp_ref, egain_ref, routes_ref, rw_ref, wg_hbm, wu_hbm, wd_hbm,
    mo_ref, eo_ref,
    wb, wc, wv, wo, wg, wu, wd, w_sem,
    gains, tables, outg,
    xg, xs, fac, outer, prod, edge, gated, pm, om, rm, sm, ym,
    xe, xes, efac, act, pe, oe, re, se, yr, fin, ra, rb, na, ny,
    mys, myr, mps, mpr, edges,
    eps, epr, eys, eyr, pps, ppr, hes, her, ses, ser, rts, rtr, nys, nyr,
    hms, hmr, yms, ymr,
):
    n_ep, n_tp, cap = dims
    chips = n_tp // 2
    n_blk = n_ep // near
    rows, feat = mix_ref.shape
    width = feat * n_tp
    half = feat * chips
    tok = exp_ref.shape[0]
    slots = n_ep * cap
    e = lax.axis_index("ep")
    t = lax.axis_index("tp")
    y, c = lax.div(t, 2), lax.rem(t, 2)
    partner = y * 2 + 1 - c
    blk, idx = lax.div(e, near), lax.rem(e, near)

    def source(p):
        return (
            lax.rem(blk + lax.div(p, near), n_blk) * near
            + lax.rem(idx + lax.rem(p, near), near)
        )

    def target(p):
        return (
            lax.rem(blk - lax.div(p, near) + n_blk, n_blk) * near
            + lax.rem(idx - lax.rem(p, near) + near, near)
        )

    def cols(b):
        return pl.ds(pl.multiple_of(b * feat, feat), feat)

    def lanes(k):
        return cols(c * chips + k)

    own_half = pl.ds(pl.multiple_of(c * half, half), half)

    def remote(src, dst, send_sem, recv_sem, ep, tp):
        return pltpu.make_async_remote_copy(
            src_ref=src, dst_ref=dst, send_sem=send_sem, recv_sem=recv_sem,
            device_id=(ep, tp), device_id_type=MESH,
        )

    def ahead(dy):
        return lax.rem(y + dy, chips)

    def peer(dy):
        return ahead(dy) * 2 + c

    def loop(first, last, body):
        lax.fori_loop(first, last, lambda i, carry: (body(i), carry)[1], 0)

    m_rows = rows // 2

    def mix_y(m, dy):
        at = pl.ds(m * m_rows, m_rows)
        return remote(
            mix_ref.at[at], xg.at[at, lanes(y)], mys.at[m, dy], myr.at[m, dy], e, peer(dy)
        )

    def mix_p(m):
        part = xg.at[pl.ds(m * m_rows, m_rows), own_half]
        return remote(part, part, mps.at[m], mpr.at[m], e, partner)

    def exp_out(p):
        return remote(outg.at[p], xe.at[p, :, lanes(y)], eps.at[p], epr.at[p], target(p), t)

    def exp_y(p, dy):
        part = xe.at[p, :, lanes(y)]
        return remote(part, part, eys.at[dy, p], eyr.at[dy, p], e, peer(dy))

    def exp_p(p):
        part = xe.at[p, :, own_half]
        return remote(part, part, pps.at[p], ppr.at[p], e, partner)

    def edge_copy():
        return remote(
            prod.at[pl.ds(rows, 8)], edge, edges.at[0], edges.at[1], lax.rem(e + 1, n_ep), t
        )

    def exp_half(j, first, last):
        at = pl.ds(first, last - first)
        return remote(pe.at[at], re.at[at], hes.at[j], her.at[j], e, partner)

    def exp_sum(p, dy):
        return remote(
            se.at[p, :, cols(ahead(dy))], yr.at[dy, p], ses.at[dy, p], ser.at[dy, p], e, peer(dy)
        )

    def near_back(p):
        return remote(se.at[p], ra.at[p], rts.at[p], rtr.at[p], source(p), t)

    def far_back(p):
        return remote(
            fin.at[p - near], rb.at[p - near], rts.at[p], rtr.at[p], source(p), t
        )

    def near_sum(dy):
        return remote(na.at[ahead(dy)], ny.at[dy], nys.at[dy], nyr.at[dy], e, peer(dy))

    def mix_half(q):
        return remote(pm.at[q], rm.at[q], hms.at[q], hmr.at[q], e, partner)

    def mix_sum(dy):
        return remote(sm.at[dy], ym.at[dy], yms.at[dy], ymr.at[dy], e, peer(dy))

    blocks = [(k, (k % chips) * 2 + k // chips) for k in range(n_tp)]

    def turned(src, dst, i):
        return [
            pltpu.make_async_copy(
                src.at[pl.ds(b * feat, feat)], dst.at[pl.ds(k * feat, feat)], w_sem.at[i, k]
            )
            for k, b in blocks
        ]

    loads = {
        "wg": turned(wg_hbm.at[0], wg, 0),
        "wu": turned(wu_hbm.at[0], wu, 1),
        "wd": [pltpu.make_async_copy(wd_hbm, wd, w_sem.at[2, 0])],
        "wc": turned(wc_hbm, wc, 3),
        "wv": turned(wv_hbm, wv, 4),
        "wb": turned(wb_hbm, wb, 5),
        "wo": [pltpu.make_async_copy(wo_hbm, wo, w_sem.at[6, 0])],
    }
    for group in loads.values():
        for load in group:
            load.start()

    def loaded(*names):
        for name in names:
            for load in loads[name]:
                load.wait()

    barrier = pltpu.get_barrier_semaphore()
    for dy in range(1, chips):
        pl.semaphore_signal(barrier, inc=1, device_id=(e, peer(dy)), device_id_type=MESH)
    pl.semaphore_signal(barrier, inc=1, device_id=(e, partner), device_id_type=MESH)

    def greet(d):
        pl.semaphore_signal(
            barrier, inc=1, device_id=(lax.rem(e + d, n_ep), t), device_id_type=MESH
        )

    loop(1, n_ep, greet)

    for k, b in blocks:
        to, at = pl.ds(k * feat, feat), pl.ds(b * feat, feat)
        gains[0:1, to] = mgain_ref[:, at]
        gains[1:2, to] = egain_ref[:, at]

    row = lax.broadcasted_iota(jnp.int32, (tok, tok), 0)
    column = lax.broadcasted_iota(jnp.int32, (tok, tok), 1)

    def upright(line):
        return jnp.sum(jnp.where(row == column, line, 0.0), axis=1, keepdims=True)

    lane_int = lax.broadcasted_iota(jnp.int32, (tok, 128), 1)
    lane = lane_int.astype(f32)
    first_slot = jnp.zeros((1, 128), f32)
    for p in range(n_ep):
        first_slot = first_slot + jnp.where(lane_int[0:1] == target(p), float(p * cap), 0.0)
    named = [upright(routes_ref[k : k + 1, :].astype(f32)) == lane for k in range(2)]
    either = jnp.where(named[0] | named[1], 1.0, 0.0).astype(bf16)
    before = row > column
    counts = jnp.dot(
        jnp.where(before, 1.0, 0.0).astype(bf16), either, preferred_element_type=f32
    )
    places = counts + first_slot
    slot_iota = lax.broadcasted_iota(jnp.int32, (tok, slots), 1).astype(f32)
    both = []
    for k in range(2):
        slot = jnp.sum(jnp.where(named[k], places, 0.0), axis=1, keepdims=True)
        one = jnp.where(slot_iota == slot, 1.0, 0.0)
        tables[k] = one.astype(bf16)
        both.append(one)
    send = (both[0] + both[1]).astype(bf16)

    outg[...] = (
        lax.dot_general(
            send, exp_ref[...], (((0,), (0,)), ((), ())), preferred_element_type=f32
        )
        .astype(bf16)
        .reshape(n_ep, cap, feat)
    )
    xe[0, :, lanes(y)] = outg[0]

    pl.semaphore_wait(barrier, n_ep - 1 + chips)

    middle = near + (n_ep - near) // 2
    parts = [(0, near), (near, middle), (middle, n_ep)]

    def pass_on(p):
        for dy in range(1, chips):
            exp_y(p, dy).start()

    def take(p):
        exp_out(p).wait_recv()
        pass_on(p)

    def relay(p):
        for dy in range(1, chips):
            exp_y(p, dy).wait_recv()
        exp_p(p).start()

    def mix_send(m):
        for dy in range(1, chips):
            mix_y(m, dy).start()

    def mix_relay(m):
        for dy in range(1, chips):
            mix_y(m, dy).wait_recv()
        mix_p(m).start()

    def scale_exp(p):
        at = pl.ds(pl.multiple_of(p * cap, cap), cap)
        exp_p(p).wait_recv()
        x = xe[p].astype(f32)
        efac[at] = lax.rsqrt(jnp.sum(x * x, axis=1, keepdims=True) / width + epsilon)
        xes[at] = (x * gains[1:2]).astype(bf16)

    hidden = wd.shape[0]
    wide_h = 256 if hidden % 256 == 0 else hidden

    def up(j):
        first, last = parts[j]
        part = pl.ds(first * cap, (last - first) * cap)
        loop(first, last, scale_exp)

        def activate(at):
            x = xes[part]
            factor = efac[part]
            gate = jnp.dot(x, wg[:, at], preferred_element_type=f32) * factor
            lift = jnp.dot(x, wu[:, at], preferred_element_type=f32) * factor
            act[part, at] = (gate / (1.0 + jnp.exp(-gate)) * lift).astype(bf16)

        if wide_h == hidden:
            activate(slice(None))
        else:
            loop(
                0, hidden // wide_h,
                lambda i: activate(pl.ds(pl.multiple_of(i * wide_h, wide_h), wide_h)),
            )

    def down(j):
        first, last = parts[j]
        part = pl.ds(first * cap, (last - first) * cap)

        def product(b, into, q):
            out = jnp.dot(act[part], wd[:, cols(b)], preferred_element_type=f32)
            into[pl.ds(first, last - first), :, cols(q)] = out.astype(bf16).reshape(
                last - first, cap, feat
            )

        loop(0, chips, lambda q: product(q * 2 + 1 - c, pe, q))
        exp_half(j, first, last).start()
        loop(0, chips, lambda q: product(q * 2 + c, oe, q))

    def joined(p, at):
        return oe[p, :, at].astype(f32) + re[p, :, at].astype(f32)

    def push_near(p):
        se[p] = joined(p, slice(None)).astype(bf16)

        @pl.when(p > 0)
        def _():
            near_back(p).start()

    def push_far(p):
        for dy in range(1, chips):
            at = cols(ahead(dy))
            se[p, :, at] = joined(p, at).astype(bf16)
            exp_sum(p, dy).start()

    def push(j):
        first, last = parts[j]
        exp_half(j, first, last).wait_recv()
        loop(first, last, push_near if first == 0 else push_far)

    def finish(p):
        whole = joined(p, cols(y))
        for dy in range(1, chips):
            exp_sum(p, dy).wait_recv()
            whole = whole + yr[dy, p].astype(f32)
        fin[p - near] = whole.astype(bf16)
        far_back(p).start()

    tile = 32

    def scale_mix(i):
        at = pl.ds(pl.multiple_of(i * tile, tile), tile)
        x = xg[at].astype(f32)
        fac[at] = lax.rsqrt(jnp.sum(x * x, axis=1, keepdims=True) / width + epsilon)
        xs[at] = (x * gains[0:1]).astype(bf16)

    wide = 256 if feat % 256 == 0 else feat

    def project(i):
        at = pl.ds(pl.multiple_of(i * wide, wide), wide)
        x = xs[...]
        factor = fac[...]
        inner = jnp.dot(x, wc[:, at], preferred_element_type=f32) * factor
        values = jnp.dot(x, wv[:, at], preferred_element_type=f32) * factor
        prod[pl.ds(8, rows), at] = inner * values
        outer[:, at] = jnp.dot(x, wb[:, at], preferred_element_type=f32) * factor

    def convolve(i):
        at = pl.ds(pl.multiple_of(i * 128, 128), 128)
        convolved = (
            conv_ref[0:1, at] * prod[pl.ds(6, rows), at]
            + conv_ref[1:2, at] * prod[pl.ds(7, rows), at]
            + conv_ref[2:3, at] * prod[pl.ds(8, rows), at]
        )
        gated[:, at] = (outer[:, at] * convolved).astype(bf16)

    def mix_down(b):
        return jnp.dot(gated[...], wo[:, cols(b)], preferred_element_type=f32).astype(bf16)

    def mix_given(q):
        pm[q] = mix_down(q * 2 + 1 - c)
        mix_half(q).start()

    def mix_kept(q):
        om[q] = mix_down(q * 2 + c)

    def mix_gates():
        for m in range(2):
            mix_p(m).wait_recv()
        loop(0, rows // tile, scale_mix)
        loaded("wc", "wv", "wb")
        loop(0, feat // wide, project)
        edge_copy().start()

    def mix_tail():
        edge_copy().wait_recv()
        prod[0:8] = jnp.where(e == 0, 0.0, edge[...])
        loop(0, feat // 128, convolve)
        loaded("wo")
        loop(0, chips, mix_given)
        loop(0, chips, mix_kept)
        for q in range(chips):
            mix_half(q).wait_recv()
        for dy in range(1, chips):
            q = ahead(dy)
            sm[dy] = (om[q].astype(f32) + rm[q].astype(f32)).astype(bf16)
            mix_sum(dy).start()

    loop(near, middle, lambda p: exp_out(p).start())
    loop(1, near, lambda p: exp_out(p).start())
    pass_on(0)
    mix_send(0)
    xg[:, lanes(y)] = mix_ref[...]
    loop(1, near, take)
    loop(near, middle, take)
    loop(middle, n_ep, lambda p: exp_out(p).start())
    mix_send(1)
    loop(0, near, relay)
    mix_relay(0)
    loaded("wg", "wu")
    up(0)
    loop(near, middle, relay)
    loaded("wd")
    down(0)
    loop(middle, n_ep, take)
    push(0)
    up(1)
    mix_relay(1)
    down(1)
    push(1)
    loop(middle, n_ep, relay)
    mix_gates()
    up(2)
    down(2)
    loop(near, middle, finish)
    push(2)
    mix_tail()
    loop(middle, n_ep, finish)

    scores = rw_ref[...]
    normalized = scores / jnp.sum(scores, axis=0, keepdims=True) * routed_scale
    share = [upright(normalized[k : k + 1, :]) for k in range(2)]

    def combine(first, last, results):
        return share[0] * jnp.dot(
            tables[0, :, first * cap : last * cap], results, preferred_element_type=f32
        ) + share[1] * jnp.dot(
            tables[1, :, first * cap : last * cap], results, preferred_element_type=f32
        )

    ra[0] = se[0]
    loop(1, near, lambda p: near_back(p).wait_recv())
    for q in range(chips):
        at = pl.ds(q * feat, feat)
        na[q] = combine(0, near, ra[:, :, at].reshape(near * cap, feat)).astype(bf16)
    for dy in range(1, chips):
        near_sum(dy).start()

    loop(near, n_ep, lambda p: far_back(p).wait_recv())
    result = combine(near, n_ep, rb[...].reshape(slots - near * cap, feat))
    result = result + na[y].astype(f32)
    for dy in range(1, chips):
        near_sum(dy).wait_recv()
        result = result + ny[dy].astype(f32)
    eo_ref[...] = result.astype(bf16)

    total = om[y].astype(f32) + rm[y].astype(f32)
    for dy in range(1, chips):
        mix_sum(dy).wait_recv()
        total = total + ym[dy].astype(f32)
    mo_ref[...] = total.astype(bf16)

    for dy in range(1, chips):
        near_sum(dy).wait_send()
        mix_sum(dy).wait_send()
        for m in range(2):
            mix_y(m, dy).wait_send()
    for m in range(2):
        mix_p(m).wait_send()
    edge_copy().wait_send()
    for q in range(chips):
        mix_half(q).wait_send()
    for j, (first, last) in enumerate(parts):
        exp_half(j, first, last).wait_send()

    def drain(p):
        exp_p(p).wait_send()
        for dy in range(1, chips):
            exp_y(p, dy).wait_send()

    def drain_out(p):
        exp_out(p).wait_send()

    def drain_far(p):
        far_back(p).wait_send()
        for dy in range(1, chips):
            exp_sum(p, dy).wait_send()

    loop(0, n_ep, drain)
    loop(1, n_ep, drain_out)
    loop(1, near, lambda p: near_back(p).wait_send())
    loop(near, n_ep, drain_far)


def solution(mesh):
    n_ep, n_tp = mesh.shape["ep"], mesh.shape["tp"]
    chips = n_tp // 2

    def local(
        mix_input, mix_gain, gate_b, gate_c, value_w, conv_weight, out_weight,
        expert_input, expert_gain, routes, route_weight, expert_gate, expert_up, expert_down,
    ):
        rows, feat = mix_input.shape
        width = feat * n_tp
        half = feat * chips
        tok, top = routes.shape
        experts = n_ep * expert_gate.shape[0]
        assert expert_gate.shape[0] == 1 and top == 2 and n_ep % near == 0
        cap = -(-(2 * tok * top // experts) // 16) * 16
        hidden = expert_gate.shape[2]
        slots = n_ep * cap
        far = n_ep - near
        vm, sem = pltpu.VMEM, pltpu.SemaphoreType.DMA
        scratch = [
            vm((width, feat), bf16), vm((width, feat), bf16), vm((width, feat), bf16),
            vm((feat, width), bf16),
            vm((width, hidden), bf16), vm((width, hidden), bf16), vm((hidden, width), bf16),
            sem((7, n_tp)),
            vm((2, width), f32), vm((2, tok, slots), bf16), vm((n_ep, cap, feat), bf16),
            vm((rows, width), bf16), vm((rows, width), bf16), vm((rows, 1), f32),
            vm((rows, feat), f32), vm((rows + 8, feat), f32), vm((8, feat), f32),
            vm((rows, feat), bf16),
            vm((chips, rows, feat), bf16), vm((chips, rows, feat), bf16),
            vm((chips, rows, feat), bf16), vm((chips, rows, feat), bf16),
            vm((chips, rows, feat), bf16),
            vm((n_ep, cap, width), bf16), vm((slots, width), bf16), vm((slots, 1), f32),
            vm((slots, hidden), bf16),
            vm((n_ep, cap, half), bf16), vm((n_ep, cap, half), bf16),
            vm((n_ep, cap, half), bf16), vm((n_ep, cap, half), bf16),
            vm((chips, n_ep, cap, feat), bf16), vm((far, cap, feat), bf16),
            vm((near, cap, half), bf16), vm((far, cap, feat), bf16),
            vm((chips, tok, feat), bf16), vm((chips, tok, feat), bf16),
            sem((2, chips)), sem((2, chips)), sem((2,)), sem((2,)), sem((2,)),
            sem((n_ep,)), sem((n_ep,)), sem((chips, n_ep)), sem((chips, n_ep)),
            sem((n_ep,)), sem((n_ep,)), sem((3,)), sem((3,)),
            sem((chips, n_ep)), sem((chips, n_ep)), sem((n_ep,)), sem((n_ep,)),
            sem((chips,)), sem((chips,)),
            sem((chips,)), sem((chips,)), sem((chips,)), sem((chips,)),
        ]
        v = pl.BlockSpec(memory_space=pltpu.VMEM)
        a = pl.BlockSpec(memory_space=pl.ANY)
        return pl.pallas_call(
            functools.partial(kernel, (n_ep, n_tp, cap)),
            out_shape=(
                jax.ShapeDtypeStruct((rows, feat), bf16),
                jax.ShapeDtypeStruct((tok, feat), bf16),
            ),
            in_specs=[v, v, a, a, a, v, a, v, v, v, v, a, a, a],
            out_specs=(v, v),
            scratch_shapes=scratch,
            compiler_params=pltpu.CompilerParams(
                collective_id=0, has_side_effects=True, vmem_limit_bytes=62 << 20
            ),
        )(
            mix_input, mix_gain.reshape(1, -1), gate_b, gate_c, value_w, conv_weight, out_weight,
            expert_input, expert_gain.reshape(1, -1), routes.T, route_weight.T,
            expert_gate, expert_up, expert_down.reshape(hidden, width),
        )

    in_specs = (
        P("ep", "tp"), P(), P(None, "tp"), P(None, "tp"), P(None, "tp"), P(None, "tp"),
        P("tp", None), P("ep", "tp"), P(), P("ep", None), P("ep", None),
        P("ep", None, "tp"), P("ep", None, "tp"), P("ep", "tp", None),
    )
    out_specs = (P("ep", "tp"), P("ep", "tp"))
    return jax.shard_map(local, mesh=mesh, in_specs=in_specs, out_specs=out_specs, check_vma=False)
```

time: 67.7 us -> 66 us (0.975)
  Pallas kernels: 63.5 us -> 61.8 us
    pallas_call x1, Pallas kernels: 63.5 us -> 61.8 us  [local(): pl.pallas_call(functools.partial(kernel, (n_ep, n_tp, cap)), out_shape=(j...]
where the time goes in v1:
time: 66 us; the launch traced here: 65.8 us
  Pallas kernels  61.8 us (94%)
  local copies, waits for them, and re-layouts  3.36 us (5%)
    pallas_call x1, Pallas kernels, local(): pl.pallas_call(functools.partial(kernel, (n_ep, n_tp, cap)), out_shape=(j...  61.8 us
    unnamed x2, local copies, waits for them, and re-layouts  3.36 us

profile of v1, /device:TPU:0, one launch (start us, length us, event | category | flops | bytes accessed | tf_op | source)
XLA Modules:
  0.0 65.8 jit_solution(4806111049671174790)
XLA Ops:
  0.6 61.8 %shard_map.149 = (bf16[384,512]{1,0:T(8,128)(2,1)}, bf16[160,512]{1,0:T(8,128)(2,1)}) custom-call(bf16[384,512]{1,0:T(8,128)(2,1)} %mix_ref.1, f32[1,2048]{1,0:T(1,128)} %bitcast.6, bf16[2048,512]{1,0:T(8,128)(2,1)} %wb_hbm.1, bf16[2048,512]{1,0:T(8,128)(2,1)} %wc_hbm.1, bf16[2048,512]{1,0:T(8,128)(2,1)} %wv_hbm.1, f32[3,512]{1,0:T(4,128)} %conv_ref.1, ...), custom_call_target="tpu_custom_call" | custom-call | tf_op jit(solution)/shard_map/pallas_call | solution.py:518
  62.4 1.8 %copy.18 = bf16[384,512]{1,0:T(8,128)(2,1)} copy(bf16[384,512]{1,0:T(8,128)(2,1)} %get-tuple-element.4) | data formatting | bytes 786432
  64.2 1.6 %copy.19 = bf16[160,512]{1,0:T(8,128)(2,1)} copy(bf16[160,512]{1,0:T(8,128)(2,1)} %get-tuple-element.5) | data formatting | bytes 327680

commit v2 on v1

--- a/solution.py
+++ b/solution.py
@@ -17,9 +17,10 @@
 
 def kernel(
     dims,
-    mix_ref, mgain_ref, wb_hbm, wc_hbm, wv_hbm, conv_ref, wo_hbm,
-    exp_ref, egain_ref, routes_ref, rw_ref, wg_hbm, wu_hbm, wd_hbm,
-    mo_ref, eo_ref,
+    mix_hbm, mgain_hbm, wb_hbm, wc_hbm, wv_hbm, conv_hbm, wo_hbm,
+    exp_hbm, egain_hbm, routes_hbm, rw_hbm, wg_hbm, wu_hbm, wd_hbm,
+    mo_hbm, eo_hbm,
+    mix_ref, mgain_ref, conv_ref, exp_ref, egain_ref, routes_ref, rw_ref, mo_ref, eo_ref, i_sem,
     wb, wc, wv, wo, wg, wu, wd, w_sem,
     gains, tables, outg,
     xg, xs, fac, outer, prod, edge, gated, pm, om, rm, sm, ym,
@@ -131,6 +132,18 @@
     def mix_sum(dy):
         return remote(sm.at[dy], ym.at[dy], yms.at[dy], ymr.at[dy], e, peer(dy))
 
+    barrier = pltpu.get_barrier_semaphore()
+    for dy in range(1, chips):
+        pl.semaphore_signal(barrier, inc=1, device_id=(e, peer(dy)), device_id_type=MESH)
+    pl.semaphore_signal(barrier, inc=1, device_id=(e, partner), device_id_type=MESH)
+
+    def greet(d):
+        pl.semaphore_signal(
+            barrier, inc=1, device_id=(lax.rem(e + d, n_ep), t), device_id_type=MESH
+        )
+
+    loop(1, n_ep, greet)
+
     blocks = [(k, (k % chips) * 2 + k // chips) for k in range(n_tp)]
 
     def turned(src, dst, i):
@@ -150,6 +163,21 @@
         "wb": turned(wb_hbm, wb, 5),
         "wo": [pltpu.make_async_copy(wo_hbm, wo, w_sem.at[6, 0])],
     }
+    small = {
+        name: pltpu.make_async_copy(src, dst, i_sem.at[i])
+        for i, (name, src, dst) in enumerate(
+            (
+                ("routes", routes_hbm, routes_ref), ("exp", exp_hbm, exp_ref),
+                ("mix", mix_hbm, mix_ref), ("mgain", mgain_hbm, mgain_ref),
+                ("egain", egain_hbm, egain_ref), ("conv", conv_hbm, conv_ref),
+                ("rw", rw_hbm, rw_ref),
+            )
+        )
+    }
+    for load in small.values():
+        load.start()
+    for load in small.values():
+        load.wait()
     for group in loads.values():
         for load in group:
             load.start()
@@ -158,23 +186,6 @@
         for name in names:
             for load in loads[name]:
                 load.wait()
-
-    barrier = pltpu.get_barrier_semaphore()
-    for dy in range(1, chips):
-        pl.semaphore_signal(barrier, inc=1, device_id=(e, peer(dy)), device_id_type=MESH)
-    pl.semaphore_signal(barrier, inc=1, device_id=(e, partner), device_id_type=MESH)
-
-    def greet(d):
-        pl.semaphore_signal(
-            barrier, inc=1, device_id=(lax.rem(e + d, n_ep), t), device_id_type=MESH
-        )
-
-    loop(1, n_ep, greet)
-
-    for k, b in blocks:
-        to, at = pl.ds(k * feat, feat), pl.ds(b * feat, feat)
-        gains[0:1, to] = mgain_ref[:, at]
-        gains[1:2, to] = egain_ref[:, at]
 
     row = lax.broadcasted_iota(jnp.int32, (tok, tok), 0)
     column = lax.broadcasted_iota(jnp.int32, (tok, tok), 1)
@@ -212,6 +223,11 @@
     )
     xe[0, :, lanes(y)] = outg[0]
 
+    for k, b in blocks:
+        to, at = pl.ds(k * feat, feat), pl.ds(b * feat, feat)
+        gains[0:1, to] = mgain_ref[:, at]
+        gains[1:2, to] = egain_ref[:, at]
+
     pl.semaphore_wait(barrier, n_ep - 1 + chips)
 
     middle = near + (n_ep - near) // 2
@@ -233,6 +249,10 @@
     def mix_send(m):
         for dy in range(1, chips):
             mix_y(m, dy).start()
+
+    def mix_sent(m):
+        for dy in range(1, chips):
+            mix_y(m, dy).wait_send()
 
     def mix_relay(m):
         for dy in range(1, chips):
@@ -249,10 +269,13 @@
     hidden = wd.shape[0]
     wide_h = 256 if hidden % 256 == 0 else hidden
 
+    def scale(j):
+        first, last = parts[j]
+        loop(first, last, scale_exp)
+
     def up(j):
         first, last = parts[j]
         part = pl.ds(first * cap, (last - first) * cap)
-        loop(first, last, scale_exp)
 
         def activate(at):
             x = xes[part]
@@ -304,6 +327,18 @@
         exp_half(j, first, last).wait_recv()
         loop(first, last, push_near if first == 0 else push_far)
 
+    def push_paced(j):
+        first, last = parts[j]
+        exp_half(j, first, last).wait_recv()
+        push_far(first)
+        for p in range(first + 1, last):
+            for dy in range(1, chips):
+                at = cols(ahead(dy))
+                se[p, :, at] = joined(p, at).astype(bf16)
+            for dy in range(1, chips):
+                exp_sum(p - 1, dy).wait_send()
+                exp_sum(p, dy).start()
+
     def finish(p):
         whole = joined(p, cols(y))
         for dy in range(1, chips):
@@ -322,14 +357,15 @@
 
     wide = 256 if feat % 256 == 0 else feat
 
-    def project(i):
+    def project(m, i):
         at = pl.ds(pl.multiple_of(i * wide, wide), wide)
-        x = xs[...]
-        factor = fac[...]
+        part = pl.ds(m * m_rows, m_rows)
+        x = xs[part]
+        factor = fac[part]
         inner = jnp.dot(x, wc[:, at], preferred_element_type=f32) * factor
         values = jnp.dot(x, wv[:, at], preferred_element_type=f32) * factor
-        prod[pl.ds(8, rows), at] = inner * values
-        outer[:, at] = jnp.dot(x, wb[:, at], preferred_element_type=f32) * factor
+        prod[pl.ds(8 + m * m_rows, m_rows), at] = inner * values
+        outer[part, at] = jnp.dot(x, wb[:, at], preferred_element_type=f32) * factor
 
     def convolve(i):
         at = pl.ds(pl.multiple_of(i * 128, 128), 128)
@@ -350,21 +386,24 @@
     def mix_kept(q):
         om[q] = mix_down(q * 2 + c)
 
-    def mix_gates():
-        for m in range(2):
-            mix_p(m).wait_recv()
-        loop(0, rows // tile, scale_mix)
-        loaded("wc", "wv", "wb")
-        loop(0, feat // wide, project)
-        edge_copy().start()
-
-    def mix_tail():
+    def mix_scale(m):
+        mix_p(m).wait_recv()
+        loop(m * m_rows // tile, (m + 1) * m_rows // tile, scale_mix)
+
+    def mix_gates(m):
+        loop(0, feat // wide, lambda i: project(m, i))
+
+    def mix_conv():
         edge_copy().wait_recv()
         prod[0:8] = jnp.where(e == 0, 0.0, edge[...])
         loop(0, feat // 128, convolve)
         loaded("wo")
+
+    def mix_dots():
         loop(0, chips, mix_given)
         loop(0, chips, mix_kept)
+
+    def mix_push():
         for q in range(chips):
             mix_half(q).wait_recv()
         for dy in range(1, chips):
@@ -374,33 +413,44 @@
 
     loop(near, middle, lambda p: exp_out(p).start())
     loop(1, near, lambda p: exp_out(p).start())
-    pass_on(0)
     mix_send(0)
     xg[:, lanes(y)] = mix_ref[...]
-    loop(1, near, take)
-    loop(near, middle, take)
+    mix_sent(0)
     loop(middle, n_ep, lambda p: exp_out(p).start())
     mix_send(1)
+    mix_relay(0)
+    mix_scale(0)
+    loop(near, middle, take)
+    loaded("wc", "wv", "wb")
+    mix_gates(0)
+    mix_relay(1)
+    loop(1, near, take)
+    pass_on(0)
+    mix_scale(1)
+    mix_gates(1)
+    edge_copy().start()
+    loop(near, middle, relay)
+    loaded("wg", "wu")
+    scale(1)
+    up(1)
+    loop(middle, n_ep, take)
+    loaded("wd")
+    down(1)
+    mix_conv()
+    push(1)
+    mix_dots()
     loop(0, near, relay)
-    mix_relay(0)
-    loaded("wg", "wu")
+    scale(0)
+    mix_push()
     up(0)
-    loop(near, middle, relay)
-    loaded("wd")
+    loop(middle, n_ep, relay)
     down(0)
-    loop(middle, n_ep, take)
+    loop(near, middle, finish)
+    scale(2)
     push(0)
-    up(1)
-    mix_relay(1)
-    down(1)
-    push(1)
-    loop(middle, n_ep, relay)
-    mix_gates()
     up(2)
     down(2)
-    loop(near, middle, finish)
     push(2)
-    mix_tail()
     loop(middle, n_ep, finish)
 
     scores = rw_ref[...]
@@ -422,6 +472,14 @@
     for dy in range(1, chips):
         near_sum(dy).start()
 
+    total = om[y].astype(f32) + rm[y].astype(f32)
+    for dy in range(1, chips):
+        mix_sum(dy).wait_recv()
+        total = total + ym[dy].astype(f32)
+    mo_ref[...] = total.astype(bf16)
+    mo_out = pltpu.make_async_copy(mo_ref, mo_hbm, i_sem.at[7])
+    mo_out.start()
+
     loop(near, n_ep, lambda p: far_back(p).wait_recv())
     result = combine(near, n_ep, rb[...].reshape(slots - near * cap, feat))
     result = result + na[y].astype(f32)
@@ -430,17 +488,15 @@
         result = result + ny[dy].astype(f32)
     eo_ref[...] = result.astype(bf16)
 
-    total = om[y].astype(f32) + rm[y].astype(f32)
-    for dy in range(1, chips):
-        mix_sum(dy).wait_recv()
-        total = total + ym[dy].astype(f32)
-    mo_ref[...] = total.astype(bf16)
+    eo_out = pltpu.make_async_copy(eo_ref, eo_hbm, i_sem.at[8])
+    eo_out.start()
+    mo_out.wait()
+    eo_out.wait()
 
     for dy in range(1, chips):
         near_sum(dy).wait_send()
         mix_sum(dy).wait_send()
-        for m in range(2):
-            mix_y(m, dy).wait_send()
+        mix_y(1, dy).wait_send()
     for m in range(2):
         mix_p(m).wait_send()
     edge_copy().wait_send()
@@ -459,6 +515,8 @@
 
     def drain_far(p):
         far_back(p).wait_send()
+
+    def drain_sum(p):
         for dy in range(1, chips):
             exp_sum(p, dy).wait_send()
 
@@ -466,6 +524,20 @@
     loop(1, n_ep, drain_out)
     loop(1, near, lambda p: near_back(p).wait_send())
     loop(near, n_ep, drain_far)
+    loop(near, n_ep, drain_sum)
+
+
+def hand_over(mix_hbm, exp_hbm, mo_hbm, eo_hbm, mix_vm, exp_vm, sems):
+    pairs = ((exp_hbm, exp_vm, eo_hbm), (mix_hbm, mix_vm, mo_hbm))
+    reads = [pltpu.make_async_copy(a, b, sems.at[0, i]) for i, (a, b, _) in enumerate(pairs)]
+    writes = [pltpu.make_async_copy(b, d, sems.at[1, i]) for i, (_, b, d) in enumerate(pairs)]
+    for read in reads:
+        read.start()
+    for read, write in zip(reads, writes):
+        read.wait()
+        write.start()
+    for write in writes:
+        write.wait()
 
 
 def solution(mesh):
@@ -488,6 +560,9 @@
         far = n_ep - near
         vm, sem = pltpu.VMEM, pltpu.SemaphoreType.DMA
         scratch = [
+            vm((rows, feat), bf16), vm((1, width), f32), vm((3, feat), f32), vm((tok, feat), bf16),
+            vm((1, width), f32), vm((2, tok), jnp.int32), vm((2, tok), f32),
+            vm((rows, feat), bf16), vm((tok, feat), bf16), sem((9,)),
             vm((width, feat), bf16), vm((width, feat), bf16), vm((width, feat), bf16),
             vm((feat, width), bf16),
             vm((width, hidden), bf16), vm((width, hidden), bf16), vm((hidden, width), bf16),
@@ -513,16 +588,16 @@
             sem((chips,)), sem((chips,)),
             sem((chips,)), sem((chips,)), sem((chips,)), sem((chips,)),
         ]
-        v = pl.BlockSpec(memory_space=pltpu.VMEM)
         a = pl.BlockSpec(memory_space=pl.ANY)
-        return pl.pallas_call(
+        outs = (
+            jax.ShapeDtypeStruct((rows, feat), bf16),
+            jax.ShapeDtypeStruct((tok, feat), bf16),
+        )
+        done = pl.pallas_call(
             functools.partial(kernel, (n_ep, n_tp, cap)),
-            out_shape=(
-                jax.ShapeDtypeStruct((rows, feat), bf16),
-                jax.ShapeDtypeStruct((tok, feat), bf16),
-            ),
-            in_specs=[v, v, a, a, a, v, a, v, v, v, v, a, a, a],
-            out_specs=(v, v),
+            out_shape=outs,
+            in_specs=[a] * 14,
+            out_specs=(a, a),
             scratch_shapes=scratch,
             compiler_params=pltpu.CompilerParams(
                 collective_id=0, has_side_effects=True, vmem_limit_bytes=62 << 20
@@ -532,6 +607,13 @@
             expert_input, expert_gain.reshape(1, -1), routes.T, route_weight.T,
             expert_gate, expert_up, expert_down.reshape(hidden, width),
         )
+        return pl.pallas_call(
+            hand_over,
+            out_shape=outs,
+            in_specs=[a, a],
+            out_specs=(a, a),
+            scratch_shapes=[vm((rows, feat), bf16), vm((tok, feat), bf16), sem((2, 2))],
+        )(*done)
 
     in_specs = (
         P("ep", "tp"), P(), P(None, "tp"), P(None, "tp"), P(None, "tp"), P(None, "tp"),

time: 66 us -> 59.5 us (0.902)
  local copies, waits for them, and re-layouts: 3.36 us -> 0 us
  Pallas kernels: 61.8 us -> 58.6 us
    unnamed x2 -> x0, local copies, waits for them, and re-layouts: 3.36 us -> none
    pallas_call x1 -> x2, Pallas kernels: 61.8 us -> 58.6 us  [the longest x1 56.8 us: local(): pl.pallas_call(functools.partial(kernel, (n_ep, n_tp, cap)), out_shape=ou...]
where the time goes in v2:
time: 59.5 us; the launch traced here: 59.3 us
  Pallas kernels  58.6 us (98%)
  between operations  0.64 us (1%)
    pallas_call x1, Pallas kernels, local(): pl.pallas_call(functools.partial(kernel, (n_ep, n_tp, cap)), out_shape=ou...  56.8 us
    pallas_call x1, Pallas kernels, local(): pl.pallas_call(hand_over, out_shape=outs, in_specs=[a, a], out_specs=(a,...  1.86 us

profile of v2, /device:TPU:0, one launch (start us, length us, event | category | flops | bytes accessed | tf_op | source)
XLA Modules:
  0.0 59.3 jit_solution(15613142062982159532)
XLA Ops:
  0.6 56.8 %shard_map.149 = (bf16[384,512]{1,0:T(8,128)(2,1)}, bf16[160,512]{1,0:T(8,128)(2,1)}) custom-call(bf16[384,512]{1,0:T(8,128)(2,1)} %mix_hbm.1, f32[1,2048]{1,0:T(1,128)} %bitcast.6, bf16[2048,512]{1,0:T(8,128)(2,1)} %wb_hbm.1, bf16[2048,512]{1,0:T(8,128)(2,1)} %wc_hbm.1, bf16[2048,512]{1,0:T(8,128)(2,1)} %wv_hbm.1, f32[3,512]{1,0:T(4,128)} %conv_hbm.1, ...), custom_call_target="tpu_custom_call" | custom-call | tf_op jit(solution)/shard_map/pallas_call | solution.py:596
  57.4 1.9 %shard_map.150 = (bf16[384,512]{1,0:T(8,128)(2,1)}, bf16[160,512]{1,0:T(8,128)(2,1)}) custom-call(bf16[384,512]{1,0:T(8,128)(2,1)} %get-tuple-element.4.mix_hbm, bf16[160,512]{1,0:T(8,128)(2,1)} %get-tuple-element.5.exp_hbm), custom_call_target="tpu_custom_call" | custom-call | tf_op jit(solution)/shard_map/pallas_call | solution.py:610

commit v3 on v2

--- a/solution.py
+++ b/solution.py
@@ -129,8 +129,11 @@
     def mix_half(q):
         return remote(pm.at[q], rm.at[q], hms.at[q], hmr.at[q], e, partner)
 
-    def mix_sum(dy):
-        return remote(sm.at[dy], ym.at[dy], yms.at[dy], ymr.at[dy], e, peer(dy))
+    def mix_sum(m, dy):
+        at = pl.ds(m * m_rows, m_rows)
+        return remote(
+            sm.at[dy, at], ym.at[dy, at], yms.at[m, dy], ymr.at[m, dy], e, peer(dy)
+        )
 
     barrier = pltpu.get_barrier_semaphore()
     for dy in range(1, chips):
@@ -214,24 +217,31 @@
         both.append(one)
     send = (both[0] + both[1]).astype(bf16)
 
-    outg[...] = (
-        lax.dot_general(
-            send, exp_ref[...], (((0,), (0,)), ((), ())), preferred_element_type=f32
-        )
-        .astype(bf16)
-        .reshape(n_ep, cap, feat)
-    )
-    xe[0, :, lanes(y)] = outg[0]
-
-    for k, b in blocks:
-        to, at = pl.ds(k * feat, feat), pl.ds(b * feat, feat)
-        gains[0:1, to] = mgain_ref[:, at]
-        gains[1:2, to] = egain_ref[:, at]
+    def select(first, last):
+        chosen = send[:, first * cap : last * cap]
+        outg[first:last] = (
+            lax.dot_general(
+                chosen, exp_ref[...], (((0,), (0,)), ((), ())), preferred_element_type=f32
+            )
+            .astype(bf16)
+            .reshape(last - first, cap, feat)
+        )
+
+    select(near, n_ep)
 
     pl.semaphore_wait(barrier, n_ep - 1 + chips)
 
     middle = near + (n_ep - near) // 2
     parts = [(0, near), (near, middle), (middle, n_ep)]
+
+    def near_send():
+        select(0, near)
+        loop(1, near, lambda p: exp_out(p).start())
+        xe[0, :, lanes(y)] = outg[0]
+        for k, b in blocks:
+            to, at = pl.ds(k * feat, feat), pl.ds(b * feat, feat)
+            gains[0:1, to] = mgain_ref[:, at]
+            gains[1:2, to] = egain_ref[:, at]
 
     def pass_on(p):
         for dy in range(1, chips):
@@ -403,30 +413,32 @@
         loop(0, chips, mix_given)
         loop(0, chips, mix_kept)
 
-    def mix_push():
-        for q in range(chips):
-            mix_half(q).wait_recv()
+    def mix_push(m):
+        at = pl.ds(m * m_rows, m_rows)
+        if m == 0:
+            for q in range(chips):
+                mix_half(q).wait_recv()
         for dy in range(1, chips):
             q = ahead(dy)
-            sm[dy] = (om[q].astype(f32) + rm[q].astype(f32)).astype(bf16)
-            mix_sum(dy).start()
+            sm[dy, at] = (om[q, at].astype(f32) + rm[q, at].astype(f32)).astype(bf16)
+            mix_sum(m, dy).start()
 
     loop(near, middle, lambda p: exp_out(p).start())
-    loop(1, near, lambda p: exp_out(p).start())
     mix_send(0)
+    near_send()
     xg[:, lanes(y)] = mix_ref[...]
     mix_sent(0)
     loop(middle, n_ep, lambda p: exp_out(p).start())
     mix_send(1)
     mix_relay(0)
     mix_scale(0)
-    loop(near, middle, take)
     loaded("wc", "wv", "wb")
     mix_gates(0)
+    loop(near, middle, take)
     mix_relay(1)
+    mix_scale(1)
     loop(1, near, take)
     pass_on(0)
-    mix_scale(1)
     mix_gates(1)
     edge_copy().start()
     loop(near, middle, relay)
@@ -440,8 +452,8 @@
     push(1)
     mix_dots()
     loop(0, near, relay)
+    mix_push(0)
     scale(0)
-    mix_push()
     up(0)
     loop(middle, n_ep, relay)
     down(0)
@@ -451,6 +463,7 @@
     up(2)
     down(2)
     push(2)
+    mix_push(1)
     loop(middle, n_ep, finish)
 
     scores = rw_ref[...]
@@ -474,7 +487,8 @@
 
     total = om[y].astype(f32) + rm[y].astype(f32)
     for dy in range(1, chips):
-        mix_sum(dy).wait_recv()
+        for m in range(2):
+            mix_sum(m, dy).wait_recv()
         total = total + ym[dy].astype(f32)
     mo_ref[...] = total.astype(bf16)
     mo_out = pltpu.make_async_copy(mo_ref, mo_hbm, i_sem.at[7])
@@ -495,7 +509,8 @@
 
     for dy in range(1, chips):
         near_sum(dy).wait_send()
-        mix_sum(dy).wait_send()
+        for m in range(2):
+            mix_sum(m, dy).wait_send()
         mix_y(1, dy).wait_send()
     for m in range(2):
         mix_p(m).wait_send()
@@ -586,7 +601,7 @@
             sem((n_ep,)), sem((n_ep,)), sem((3,)), sem((3,)),
             sem((chips, n_ep)), sem((chips, n_ep)), sem((n_ep,)), sem((n_ep,)),
             sem((chips,)), sem((chips,)),
-            sem((chips,)), sem((chips,)), sem((chips,)), sem((chips,)),
+            sem((chips,)), sem((chips,)), sem((2, chips)), sem((2, chips)),
         ]
         a = pl.BlockSpec(memory_space=pl.ANY)
         outs = (

time: 59.5 us -> 58.4 us (0.982)
  Pallas kernels: 58.6 us -> 57.6 us
    pallas_call x1, Pallas kernels: 56.8 us -> 55.7 us  [local(): pl.pallas_call(functools.partial(kernel, (n_ep, n_tp, cap)), out_shape=ou...]
where the time goes in v3:
time: 58.4 us; the launch traced here: 58.2 us
  Pallas kernels  57.6 us (99%)
  between operations  0.64 us (1%)
    pallas_call x1, Pallas kernels, local(): pl.pallas_call(functools.partial(kernel, (n_ep, n_tp, cap)), out_shape=ou...  55.7 us
    pallas_call x1, Pallas kernels, local(): pl.pallas_call(hand_over, out_shape=outs, in_specs=[a, a], out_specs=(a,...  1.86 us

profile of v3, /device:TPU:0, one launch (start us, length us, event | category | flops | bytes accessed | tf_op | source)
XLA Modules:
  0.0 58.2 jit_solution(12783160168367889034)
XLA Ops:
  0.6 55.7 %shard_map.149 = (bf16[384,512]{1,0:T(8,128)(2,1)}, bf16[160,512]{1,0:T(8,128)(2,1)}) custom-call(bf16[384,512]{1,0:T(8,128)(2,1)} %mix_hbm.1, f32[1,2048]{1,0:T(1,128)} %bitcast.6, bf16[2048,512]{1,0:T(8,128)(2,1)} %wb_hbm.1, bf16[2048,512]{1,0:T(8,128)(2,1)} %wc_hbm.1, bf16[2048,512]{1,0:T(8,128)(2,1)} %wv_hbm.1, f32[3,512]{1,0:T(4,128)} %conv_hbm.1, ...), custom_call_target="tpu_custom_call" | custom-call | tf_op jit(solution)/shard_map/pallas_call | solution.py:611
  56.3 1.9 %shard_map.150 = (bf16[384,512]{1,0:T(8,128)(2,1)}, bf16[160,512]{1,0:T(8,128)(2,1)}) custom-call(bf16[384,512]{1,0:T(8,128)(2,1)} %get-tuple-element.4.mix_hbm, bf16[160,512]{1,0:T(8,128)(2,1)} %get-tuple-element.5.exp_hbm), custom_call_target="tpu_custom_call" | custom-call | tf_op jit(solution)/shard_map/pallas_call | solution.py:625

commit v4 on v3

--- a/solution.py
+++ b/solution.py
@@ -445,15 +445,15 @@
     loaded("wg", "wu")
     scale(1)
     up(1)
-    loop(middle, n_ep, take)
     loaded("wd")
     down(1)
+    loop(middle, n_ep, take)
     mix_conv()
     push(1)
     mix_dots()
     loop(0, near, relay)
+    scale(0)
     mix_push(0)
-    scale(0)
     up(0)
     loop(middle, n_ep, relay)
     down(0)

time: 58.4 us -> 58.4 us (level)
  no operation moved by 1% of the time
where the time goes in v4:
time: 58.4 us; the launch traced here: 58.2 us
  Pallas kernels  57.6 us (99%)
  between operations  0.64 us (1%)
    pallas_call x1, Pallas kernels, local(): pl.pallas_call(functools.partial(kernel, (n_ep, n_tp, cap)), out_shape=ou...  55.7 us
    pallas_call x1, Pallas kernels, local(): pl.pallas_call(hand_over, out_shape=outs, in_specs=[a, a], out_specs=(a,...  1.86 us

profile of v4, /device:TPU:0, one launch (start us, length us, event | category | flops | bytes accessed | tf_op | source)
XLA Modules:
  0.0 58.2 jit_solution(17032082514695211504)
XLA Ops:
  0.6 55.7 %shard_map.149 = (bf16[384,512]{1,0:T(8,128)(2,1)}, bf16[160,512]{1,0:T(8,128)(2,1)}) custom-call(bf16[384,512]{1,0:T(8,128)(2,1)} %mix_hbm.1, f32[1,2048]{1,0:T(1,128)} %bitcast.6, bf16[2048,512]{1,0:T(8,128)(2,1)} %wb_hbm.1, bf16[2048,512]{1,0:T(8,128)(2,1)} %wc_hbm.1, bf16[2048,512]{1,0:T(8,128)(2,1)} %wv_hbm.1, f32[3,512]{1,0:T(4,128)} %conv_hbm.1, ...), custom_call_target="tpu_custom_call" | custom-call | tf_op jit(solution)/shard_map/pallas_call | solution.py:611
  56.4 1.9 %shard_map.150 = (bf16[384,512]{1,0:T(8,128)(2,1)}, bf16[160,512]{1,0:T(8,128)(2,1)}) custom-call(bf16[384,512]{1,0:T(8,128)(2,1)} %get-tuple-element.4.mix_hbm, bf16[160,512]{1,0:T(8,128)(2,1)} %get-tuple-element.5.exp_hbm), custom_call_target="tpu_custom_call" | custom-call | tf_op jit(solution)/shard_map/pallas_call | solution.py:625
